TPU v7x, 32 devices: a whole 2x2x4 slice. The times are simulated.
32 devices in a mesh: sp: 16 (over z, y, x), tp: 2 (over core).
Axes of the slice: x: 2, y: 2, z: 4, core: 2. Of those that a mesh axis runs over, the one named last changes fastest.
Arguments:
- glu_value: bfloat16 [4096, 1024], P('sp', 'tp'), may hold values from -12 to 12
- glu_gate: bfloat16 [4096, 1024], P('sp', 'tp'), may hold values from -8 to 8
- conv_kernel: bfloat16 [31, 1024], P(None, 'tp'), may hold values from -1 to 1
- conv_bias: float32 [1024], P('tp'), may hold values from -1.5 to 1.5
- group_gain: float32 [1024], P('tp'), may hold values from 0.1 to 1.9
- group_shift: float32 [1024], P('tp'), may hold values from -2.5 to 2.5
- out_weight: bfloat16 [1024, 2048], replicated, may hold values from -0.1875 to 0.1875
- residual: bfloat16 [4096, 2048], P(('sp', 'tp')), may hold values from -12 to 12
- ffn_gain: float32 [2048], replicated, may hold values from 0.1 to 1.9
- expert_pick: int32 [4096, 2], P(('sp', 'tp')), may hold values from 0 to 31, as said below
- pair_logits: float32 [4096, 2], P(('sp', 'tp')), may hold values from -1.2 to 1.2
- group_prob: float32 [4096], P(('sp', 'tp')), may hold values from 0.5 to 1
- gate_weight: bfloat16 [32, 2048, 512], P(('sp', 'tp')), may hold values from -0.125 to 0.125
- up_weight: bfloat16 [32, 2048, 512], P(('sp', 'tp')), may hold values from -0.125 to 0.125
- down_weight: bfloat16 [32, 512, 2048], P(('sp', 'tp')), may hold values from -0.75 to 0.75
Outputs:
- result: bfloat16 [4096, 2048], P(('sp', 'tp'))
Inputs may be any that keep to these rules, and one draw needn't show every extreme that they name: `expert_pick`: both picks of a token are different experts of the same group of 8 consecutive experts. Among the 128 tokens of one device (aligned blocks of rows) no expert is picked more than 16 times, and in every such block some expert is picked exactly 16 times.
All inputs are finite; a program needn't handle non-finite values.
Results may differ from a plain program's by a relative error of at most 0.014.
Values may be sent and summed in bfloat16 or wider, within the bound.
A program may use at most 64 MiB of HBM per device.

v0:
```python
import jax
import jax.numpy as jnp
from jax import lax
from jax.sharding import PartitionSpec as P

CONV_GROUPS = 8


EPS = 1e-06


def from_behind(value, axis, by):
    peers = lax.axis_size(axis)
    pairs = [(i, i + by) for i in range(peers) if 0 <= i + by < peers]
    return lax.ppermute(value, axis, pairs)


def local(
    glu_value,
    glu_gate,
    conv_kernel,
    conv_bias,
    group_gain,
    group_shift,
    out_weight,
    residual,
    ffn_gain,
    expert_pick,
    pair_logits,
    group_prob,
    gate_weight,
    up_weight,
    down_weight,
):
    glued_rows = (
        glu_value.astype(jnp.float32) * jax.nn.sigmoid(glu_gate.astype(jnp.float32))
    ).astype(jnp.bfloat16)
    reach_rows = conv_kernel.shape[0] - 1
    length = glued_rows.shape[0]
    earlier = from_behind(glued_rows[length - reach_rows :], "sp", 1)
    extended = jnp.concatenate([earlier, glued_rows], axis=0).astype(jnp.float32)
    kernel = conv_kernel.astype(jnp.float32)
    summed = jnp.zeros(glued_rows.shape, jnp.float32) + conv_bias
    for offset in range(reach_rows + 1):
        summed = summed + kernel[offset] * extended[offset : offset + length]
    groups_here = CONV_GROUPS // lax.axis_size("tp")
    grouped = summed.reshape(length, groups_here, -1)
    centre = jnp.mean(grouped, axis=-1, keepdims=True)
    variance = jnp.mean(jnp.square(grouped - centre), axis=-1, keepdims=True)
    leveled = ((grouped - centre) * lax.rsqrt(variance + EPS)).reshape(length, -1)
    mixed_rows = jax.nn.silu(leveled * group_gain + group_shift).astype(jnp.bfloat16)
    local_rows = residual.shape[0]
    regrouped = lax.all_to_all(mixed_rows, "tp", split_axis=0, concat_axis=1, tiled=True)
    projected = jnp.dot(regrouped, out_weight, preferred_element_type=jnp.float32)
    hidden = (residual.astype(jnp.float32) + projected).astype(jnp.bfloat16)
    hidden_full = hidden.astype(jnp.float32)
    scale_rows = lax.rsqrt(jnp.mean(hidden_full * hidden_full, axis=-1, keepdims=True) + EPS)
    normed = (hidden_full * scale_rows * ffn_gain).astype(jnp.bfloat16)
    experts_all = lax.axis_size("sp") * lax.axis_size("tp")
    capacity = 4 * local_rows // experts_all
    picks = expert_pick.shape[1]
    model_width = normed.shape[1]
    slot_experts = expert_pick.reshape(-1)
    onehot = (slot_experts[:, None] == jnp.arange(experts_all, dtype=jnp.int32)[None, :]).astype(
        jnp.int32
    )
    before = jnp.cumsum(onehot, axis=0) - onehot
    slot_rank = jnp.sum(before * onehot, axis=1)
    slot_place = slot_experts * capacity + slot_rank
    doubled = jnp.repeat(normed, picks, axis=0)
    outgoing = (
        jnp.zeros((experts_all * capacity, model_width), jnp.bfloat16).at[slot_place].set(doubled)
    )
    outgoing = outgoing.reshape(experts_all, capacity, model_width)
    arrived = lax.all_to_all(outgoing, ("sp", "tp"), split_axis=0, concat_axis=0, tiled=True)
    senders, slot_count, width_here = arrived.shape
    flat_rows = arrived.reshape(senders * slot_count, width_here)
    gate_out = jnp.dot(flat_rows, gate_weight[0], preferred_element_type=jnp.float32)
    up_out = jnp.dot(flat_rows, up_weight[0], preferred_element_type=jnp.float32)
    active = (jax.nn.silu(gate_out) * up_out).astype(jnp.bfloat16)
    answer = jnp.dot(active, down_weight[0], preferred_element_type=jnp.float32).astype(
        jnp.bfloat16
    )
    returned = lax.all_to_all(
        answer.reshape(senders, slot_count, width_here),
        ("sp", "tp"),
        split_axis=0,
        concat_axis=0,
        tiled=True,
    )
    flat_returned = returned.reshape(experts_all * capacity, model_width)
    picked = flat_returned[slot_place].reshape(local_rows, picks, model_width)
    first_share = group_prob * jax.nn.sigmoid(pair_logits[:, 0] - pair_logits[:, 1])
    second_share = group_prob * jax.nn.sigmoid(pair_logits[:, 1] - pair_logits[:, 0])
    combined = hidden_full + first_share[:, None] * picked[:, 0].astype(jnp.float32)
    combined = combined + second_share[:, None] * picked[:, 1].astype(jnp.float32)
    return combined.astype(jnp.bfloat16)


def solution(mesh):
    in_specs = (
        P("sp", "tp"),
        P("sp", "tp"),
        P(None, "tp"),
        P("tp"),
        P("tp"),
        P("tp"),
        P(),
        P(("sp", "tp"), None),
        P(),
        P(("sp", "tp"), None),
        P(("sp", "tp"), None),
        P(("sp", "tp")),
        P(("sp", "tp"), None, None),
        P(("sp", "tp"), None, None),
        P(("sp", "tp"), None, None),
    )
    out_specs = P(("sp", "tp"), None)
    return jax.shard_map(local, mesh=mesh, in_specs=in_specs, out_specs=out_specs, check_vma=False)
```

profile of v0, /device:TPU:0, one launch (start us, length us, event | category | flops | bytes accessed | tf_op | source)
XLA Modules:
  0.0 159.1 jit_solution(16417877492611930795)
XLA Ops:
  0.0 0.0 copy-start
  0.0 0.0 copy-start.6
  0.0 1.3 multiply_convert_fusion.2
  1.4 4.9 %collective-permute-start = (bf16[30,512]{1,0:T(8,128)(2,1)S(1)}, bf16[30,512]{1,0:T(8,128)(2,1)S(1)}, u32[]{:S(2)}, u32[]{:S(2)}) collective-permute-start(bf16[30,512]{1,0:T(8,128)(2,1)S(1)} %slice.281), channel_id=1, source_target_pairs={{0,2},{2,4},{4,6},{6,8},{8,10},{10,12},{12,14},{14,16},{16,18},{18... | collective-permute-start | bytes 92168 | tf_op jit(solution)/shard_map/ppermute | solution.py:15
  6.2 1.0 fusion.60
  7.3 1.0 fusion.61
  8.3 0.8 copy.24
  9.1 0.1 eq.29
  9.2 0.1 eq.25
  9.3 0.7 broadcast_multiply_fusion.1
  10.0 0.6 reduce-window.6
  10.6 0.2 slice_reduce_fusion
  10.9 0.1 copy.23
  11.0 0.1 mul.507
  11.1 0.1 fusion.56
  11.2 0.0 collective-permute-done
  11.2 0.1 maximum_convert_fusion
  11.3 0.0 copy-done.6
  11.3 2.8 %fusion.22 = f32[256,512]{1,0:T(8,128)} fusion(f32[286,512]{1,0:T(8,128)S(1)} %maximum_convert_fusion, f32[512]{0:T(512)S(1)} %bitcast.177, f32[512]{0:T(512)S(1)} %bitcast.175, f32[512]{0:T(512)S(1)} %bitcast.173, f32[512]{0:T(512)S(1)} %bitcast.171, f32[512]{0:T(512)S(1)} %bitcast.169, f32[512]{0:T(512)S(1)} %bitcast.167, f32[512]{0:T(512)S(1)} %bitcast.165, ...), kind=kLoop, calls=%fused_computation.27 | loop fusion | flops 8126464 | bytes 16842752 | tf_op jit(solution)/shard_map/add | solution.py:45
  14.1 0.0 copy-start.7
  14.1 0.0 copy-start.8
  14.1 1.2 reshape.113
  15.4 0.3 reduce_sum.38
  15.7 0.6 multiply_reduce_fusion.1
  16.4 0.3 mul.497
  16.7 0.3 sub.28
  17.1 0.0 copy-done.7
  17.1 0.0 copy-done.8
  17.1 0.0 copy-start.4
  17.1 2.3 %multiply_convert_fusion.1 = bf16[256,512]{1,0:T(8,128)(2,1)S(1)} fusion(f32[32,8,4,128]{3,2,1,0:T(4,128)S(1)} %bitcast.109, f32[32,8,4,128]{3,2,1,0:T(4,128)S(1)} %bitcast.110, f32[512]{0:T(512)S(1)} %copy-done.7, f32[512]{0:T(512)S(1)} %copy-done.8, f32[286,512]{1,0:T(8,128)S(1)} %maximum_convert_fusion, f32[512]{0:T(512)S(1)} %bitcast.178, ...), kind=kLoop, calls=%fused_computation.91 | loop fusion | flops 9306112 | bytes 17633280 | tf_op jit(solution)/shard_map/convert_element_type | solution.py:51
  19.4 3.9 %all_to_all.29 = bf16[2,128,512]{2,1,0:T(8,128)(2,1)S(1)} all-to-all(bf16[2,128,512]{2,1,0:T(8,128)(2,1)S(1)} %bitcast.114), channel_id=1, replica_groups=mesh['sp'=16,'tp'=2] {'tp'}, dimensions={0} | all-to-all | bytes 524288 | tf_op jit(solution)/shard_map/all_to_all | solution.py:53
  23.4 0.2 copy.22
  23.5 0.0 copy-done.4
  23.6 0.0 copy-start.5
  23.6 3.0 %multiply_reduce_fusion = (f32[128]{0:T(128)S(1)}, f32[128,2048]{1,0:T(8,128)S(1)}) fusion(bf16[128,1024]{0,1:T(8,128)(2,1)S(1)} %bitcast.115, bf16[1024,2048]{1,0:T(8,128)(2,1)} %param.21, bf16[128,2048]{1,0:T(8,128)(2,1)S(1)} %copy-done.4), kind=kOutput, calls=%fused_computation.19 | convolution fusion | flops 538443648 | bytes 6029824 | tf_op jit(solution)/shard_map/dot_general | solution.py:54
  26.6 0.0 copy-start.1
  26.6 1.0 copy-done.1
  27.6 0.0 copy-done.5
  27.6 0.2 multiply_convert_fusion
  27.7 0.6 broadcast_in_dim.5
  28.4 1.2 reshape.139
  29.6 4.4 %scatter_custom_fusion = bf16[512,2048]{1,0:T(8,128)(2,1)} fusion(s32[256]{0:T(256)S(1)} %bitcast.179, bf16[256,2048]{1,0:T(8,128)(2,1)} %reshape.139, bf16[]{:T(256)} %constant.8.clone.1), kind=kCustom, calls=%fused_computation.20 | custom fusion | bytes 2097664 | tf_op jit(solution)/shard_map/scatter | solution.py:72
  34.0 0.0 copy-start.11
  34.0 53.6 %all_to_all.30 = bf16[32,16,2048]{2,1,0:T(8,128)(2,1)S(1)} all-to-all(bf16[32,16,2048]{2,1,0:T(8,128)(2,1)} %bitcast.108), channel_id=1, replica_groups=mesh['sp'=16,'tp'=2] {'sp','tp'}, dimensions={0} | all-to-all | bytes 4194304 | tf_op jit(solution)/shard_map/all_to_all | solution.py:75
  87.6 0.0 copy-start.3
  87.6 1.3 copy-done.3
  89.0 0.0 copy-done.11
  89.0 1.2 fusion.5
  90.2 0.0 copy-done
  90.3 6.0 %convolution_convert_fusion = bf16[512,2048]{1,0:T(8,128)(2,1)} fusion(bf16[1,512,2048]{2,1,0:T(8,128)(2,1)S(1)} %copy-done, bf16[512,2048]{1,0:T(8,128)(2,1)} %bitcast.113, bf16[1,2048,512]{2,1,0:T(8,128)(2,1)} %param.28, f32[512,512]{1,0:T(8,128)S(1)} %fusion.5), kind=kOutput, calls=%fused_computation.2 | convolution fusion | flops 2150105088 | bytes 9437184 | tf_op jit(solution)/shard_map/dot_general | solution.py:81
  96.2 0.0 copy-start.9
  96.2 0.0 copy-start.10
  96.2 3.8 %all-to-all-start.2 = ((bf16[32,16,2048]{2,1,0:T(8,128)(2,1)}), bf16[32,16,2048]{2,1,0:T(8,128)(2,1)}, u32[]{:S(2)}, u32[]{:S(2)}) async-start(bf16[32,16,2048]{2,1,0:T(8,128)(2,1)} %bitcast.111), calls=%async_computation.2 | async-start | bytes 4194304 | tf_op jit(solution)/shard_map/all_to_all | solution.py:84
  100.0 0.0 copy-done.9
  100.0 0.0 copy-done.10
  100.1 48.7 %all-to-all-done.2 = bf16[32,16,2048]{2,1,0:T(8,128)(2,1)} async-done(((bf16[32,16,2048]{2,1,0:T(8,128)(2,1)}), bf16[32,16,2048]{2,1,0:T(8,128)(2,1)}, u32[]{:S(2)}, u32[]{:S(2)}) %all-to-all-start.2) | async-done | bytes 2097184 | tf_op jit(solution)/shard_map/all_to_all | solution.py:84
  148.7 5.2 %gather_fusion = bf16[256,2048]{1,0:T(8,128)(2,1)} fusion(bf16[512,2048]{1,0:T(8,128)(2,1)} %bitcast.44, s32[1024]{0:T(1024)S(1)} %pad_clamp_fusion), kind=kCustom, calls=%fused_computation | custom fusion | bytes 2098176 | tf_op jit(solution)/shard_map/gather | solution.py:92
  153.9 1.7 %reshape.120 = bf16[128,2,2048]{2,1,0:T(2,128)(2,1)S(1)} reshape(bf16[256,2048]{1,0:T(8,128)(2,1)} %gather_fusion) | data formatting | bytes 2097152 | tf_op jit(solution)/shard_map/reshape | solution.py:92
  155.7 0.0 copy-start.2
  155.7 1.5 fusion.59
  157.2 0.0 copy-done.2
  157.2 1.9 %fusion.14 = bf16[128,2048]{1,0:T(8,128)(2,1)} fusion(f32[128,2048]{1,0:T(8,128)S(1)} %copy-done.2, bf16[128,1,2048]{2,1,0:T(2,128)(2,1)S(1)} %get-tuple-element.6, bf16[128,1,2048]{2,1,0:T(2,128)(2,1)S(1)} %get-tuple-element.5, f32[128]{0:T(128)S(1)} %get-tuple-element.39, f32[128]{0:T(128)S(1)} %get-tuple-element.38), kind=kLoop, calls=%fused_computation.15 | loop fusion | flops 1835008 | bytes 2622464 | tf_op jit(solution)/shard_map/convert_element_type | solution.py:97
  (10 shorter events, 0.1 us)
Async XLA Ops:
  0.0 90.2 %copy-start = (bf16[1,512,2048]{2,1,0:T(8,128)(2,1)S(1)}, bf16[1,512,2048]{2,1,0:T(8,128)(2,1)}, u32[]{:S(2)}) copy-start(bf16[1,512,2048]{2,1,0:T(8,128)(2,1)} %param.29) | copy-start | bytes 6291460
  0.0 11.3 %copy-start.6 = (f32[512]{0:T(512)S(1)}, f32[512]{0:T(512)}, u32[]{:S(2)}) copy-start(f32[512]{0:T(512)} %param.18) | copy-start | bytes 6148
  1.4 9.9 %collective-permute-start = (bf16[30,512]{1,0:T(8,128)(2,1)S(1)}, bf16[30,512]{1,0:T(8,128)(2,1)S(1)}, u32[]{:S(2)}, u32[]{:S(2)}) collective-permute-start(bf16[30,512]{1,0:T(8,128)(2,1)S(1)} %slice.281), channel_id=1, source_target_pairs={{0,2},{2,4},{4,6},{6,8},{8,10},{10,12},{12,14},{14,16},{16,18},{18... | collective-permute-start | bytes 92168 | tf_op jit(solution)/shard_map/ppermute | solution.py:15
  14.1 3.0 %copy-start.7 = (f32[512]{0:T(512)S(1)}, f32[512]{0:T(512)}, u32[]{:S(2)}) copy-start(f32[512]{0:T(512)} %param.20) | copy-start | bytes 6148
  14.1 3.0 %copy-start.8 = (f32[512]{0:T(512)S(1)}, f32[512]{0:T(512)}, u32[]{:S(2)}) copy-start(f32[512]{0:T(512)} %param.19) | copy-start | bytes 6148
  17.1 6.4 %copy-start.4 = (bf16[128,2048]{1,0:T(8,128)(2,1)S(1)}, bf16[128,2048]{1,0:T(8,128)(2,1)}, u32[]{:S(2)}) copy-start(bf16[128,2048]{1,0:T(8,128)(2,1)} %param.22) | copy-start | bytes 1572868
  23.6 4.0 %copy-start.5 = (f32[2048]{0:T(1024)S(1)}, f32[2048]{0:T(1024)}, u32[]{:S(2)}) copy-start(f32[2048]{0:T(1024)} %param.23) | copy-start | bytes 24580
  26.6 1.0 copy-start.1
  34.0 55.0 %copy-start.11 = (bf16[1,2048,512]{2,1,0:T(8,128)(2,1)S(1)}, bf16[1,2048,512]{2,1,0:T(8,128)(2,1)}, u32[]{:S(2)}) copy-start(bf16[1,2048,512]{2,1,0:T(8,128)(2,1)} %param.27) | copy-start | bytes 6291460
  87.6 1.4 copy-start.3
  96.2 3.8 %copy-start.9 = (f32[128,2]{0,1:T(2,128)S(1)}, f32[128,2]{0,1:T(2,128)}, u32[]{:S(2)}) copy-start(f32[128,2]{0,1:T(2,128)} %param.25) | copy-start | bytes 3076
  96.2 3.8 %copy-start.10 = (f32[128]{0:T(128)S(1)}, f32[128]{0:T(128)}, u32[]{:S(2)}) copy-start(f32[128]{0:T(128)} %param.26) | copy-start | bytes 1540
  96.2 52.5 %all-to-all-start.2 = ((bf16[32,16,2048]{2,1,0:T(8,128)(2,1)}), bf16[32,16,2048]{2,1,0:T(8,128)(2,1)}, u32[]{:S(2)}, u32[]{:S(2)}) async-start(bf16[32,16,2048]{2,1,0:T(8,128)(2,1)} %bitcast.111), calls=%async_computation.2 | async-start | bytes 4194304 | tf_op jit(solution)/shard_map/all_to_all | solution.py:84
  155.7 1.5 copy-start.2
where the time goes:
time: 160 us; the launch traced here: 159 us
  blocking collectives  57.5 us (36%)
  waiting for transfers between devices  48.7 us (30%)
  local copies, waits for them, and re-layouts  22.7 us (14%)
  other arithmetic  11 us (7%)
  matrix products  10.2 us (6%)
  starting transfers between devices  8.67 us (5%)
    all_to_all x1, blocking collectives, local(): lax.all_to_all(outgoing, ('sp', 'tp'), split_axis=0, concat_axis=0, tiled...  53.6 us
    all_to_all x1, waiting for transfers between devices, local(): lax.all_to_all(answer.reshape(senders, slot_count, width_here), ('sp', 't...  48.7 us
    dot_general x1, matrix products, local(): jnp.dot(active, down_weight[0], preferred_element_type=jnp.float32)  5.96 us
    gather x1, local copies, waits for them, and re-layouts, local(): picked = flat_returned[slot_place].reshape(local_rows, picks, model_width)  5.21 us
    ppermute x1, starting transfers between devices, from_behind(): return lax.ppermute(value, axis, pairs)  4.87 us
    scatter x1, local copies, waits for them, and re-layouts, local(): jnp.zeros((experts_all * capacity, model_width), jnp.bfloat16)  4.43 us
    all_to_all x1, blocking collectives, local(): lax.all_to_all(mixed_rows, 'tp', split_axis=0, concat_axis=1, tiled=True)  3.94 us
    all_to_all x1, starting transfers between devices, local(): lax.all_to_all(answer.reshape(senders, slot_count, width_here), ('sp', 't...  3.79 us
  transfers between devices with their start and end apart: 2, of which 1 were waited for; matrix products, arithmetic and copies ran while one was open for 3% of the time, Pallas kernels for 0%

commit v1 on v0

v1 whole, which is shorter than its diff:
```python
import functools

import jax
import jax.numpy as jnp
from jax import lax
from jax.experimental import pallas as pl
from jax.experimental.pallas import tpu as pltpu
from jax.sharding import PartitionSpec as P

CONV_GROUPS = 8


EPS = 1e-06


def from_behind(value, axis, by):
    peers = lax.axis_size(axis)
    pairs = [(i, i + by) for i in range(peers) if 0 <= i + by < peers]
    return lax.ppermute(value, axis, pairs)

PLANES = 4
MESH = pl.DeviceIdType.MESH
ORDER = (1, 3, 2)
ROWS_MIN = 16


def moe_kernel(
    cap,
    slot,
    normed_ref,
    hidden_ref,
    place_ref,
    meta_ref,
    gate_hbm,
    up_hbm,
    down_hbm,
    out_ref,
    zsend,
    zrecv,
    mrecv,
    xsend,
    xrecv,
    asend,
    arecv,
    csend,
    cret,
    gate_v,
    up_v,
    down_v,
    wsem,
    zss,
    zrs,
    mss,
    mrs,
    xss,
    xrs,
    ass,
    ars,
    css,
    crs,
):
    n_tp = lax.axis_size("tp")
    chips = lax.axis_size("sp") // PLANES
    peers = chips * n_tp
    sp = lax.axis_index("sp")
    tp = lax.axis_index("tp")
    z = sp // chips
    here = sp % chips
    j = here * n_tp + tp
    slots = peers * slot
    group_rows = zsend.shape[1]

    def plane(d):
        if d == 1:
            return z + 1 - 2 * (z % 2)
        if d == 2:
            return z + 2 - 4 * (z // 2)
        return PLANES - 1 - z

    def mate(d):
        return (plane(d) * chips + here, tp)

    def peer(k):
        return (z * chips + k // n_tp, k % n_tp)

    def zcopy(d):
        return pltpu.make_async_remote_copy(
            src_ref=zsend.at[d], dst_ref=zrecv.at[d], send_sem=zss.at[d], recv_sem=zrs.at[d],
            device_id=mate(d), device_id_type=MESH,
        )

    def mcopy(d):
        return pltpu.make_async_remote_copy(
            src_ref=meta_ref.at[d], dst_ref=mrecv.at[d], send_sem=mss.at[d], recv_sem=mrs.at[d],
            device_id=mate(d), device_id_type=MESH,
        )

    def ccopy(d):
        return pltpu.make_async_remote_copy(
            src_ref=csend.at[d], dst_ref=cret.at[d], send_sem=css.at[d], recv_sem=crs.at[d],
            device_id=mate(d), device_id_type=MESH,
        )

    def xcopy(d, o):
        rows = pl.ds(o * slot, slot)
        return pltpu.make_async_remote_copy(
            src_ref=xsend.at[d, rows], dst_ref=xrecv.at[d, rows],
            send_sem=xss.at[d, o], recv_sem=xrs.at[d, o],
            device_id=peer((j + o) % peers), device_id_type=MESH,
        )

    def acopy(d, o):
        rows = pl.ds(o * slot, slot)
        return pltpu.make_async_remote_copy(
            src_ref=asend.at[d, rows], dst_ref=arecv.at[d, rows],
            send_sem=ass.at[d, o], recv_sem=ars.at[d, o],
            device_id=peer((j + peers - o) % peers), device_id_type=MESH,
        )

    weights = [
        pltpu.make_async_copy(gate_hbm.at[0], gate_v, wsem.at[0]),
        pltpu.make_async_copy(up_hbm.at[0], up_v, wsem.at[1]),
        pltpu.make_async_copy(down_hbm.at[0], down_v, wsem.at[2]),
    ]
    for copy in weights:
        copy.start()

    barrier = pltpu.get_barrier_semaphore()
    for d in ORDER:
        pl.semaphore_signal(barrier, inc=1, device_id=mate(d), device_id_type=MESH)
    for o in range(1, peers):
        pl.semaphore_signal(
            barrier, inc=1, device_id=peer((j + o) % peers), device_id_type=MESH
        )
    for d in (0,) + ORDER:
        picked = jnp.dot(
            place_ref[d * group_rows : (d + 1) * group_rows, :],
            normed_ref[...],
            preferred_element_type=jnp.float32,
        )
        zsend[d] = picked.astype(jnp.bfloat16)
    pl.semaphore_wait(barrier, len(ORDER) + peers - 1)
    for d in ORDER:
        mcopy(d).start()
    for d in ORDER:
        zcopy(d).start()

    def places(d):
        meta = meta_ref[0] if d == 0 else mrecv[d]
        row = lax.broadcasted_iota(jnp.int32, (slots, group_rows), 0).astype(jnp.float32)
        shift = (j * slot).astype(jnp.float32)
        out = []
        for k in range(2):
            at = meta[k : k + 1, :group_rows] - shift
            at = jnp.where(at < 0, at + slots, at)
            out.append(row == at)
        shares = [meta[2 + k : 3 + k, :group_rows] for k in range(2)]
        return out, shares

    def entry(d):
        if d:
            mcopy(d).wait_recv()
            zcopy(d).wait_recv()
        at, _ = places(d)
        chosen = jnp.where(at[0] | at[1], 1.0, 0.0).astype(jnp.bfloat16)
        rows = zsend[0] if d == 0 else zrecv[d]
        spread = jnp.dot(chosen, rows, preferred_element_type=jnp.float32).astype(jnp.bfloat16)
        xrecv[d, :slot] = spread[:slot]
        xsend[d, slot:] = spread[slot:]
        for o in range(1, peers):
            xcopy(d, o).start()

    def expert(d):
        for o in range(1, peers):
            xcopy(d, o).wait_recv()
        rows = xrecv[d]
        gate_out = jnp.dot(rows, gate_v[...], preferred_element_type=jnp.float32)
        up_out = jnp.dot(rows, up_v[...], preferred_element_type=jnp.float32)
        active = (gate_out / (1.0 + jnp.exp(-gate_out)) * up_out).astype(jnp.bfloat16)
        answer = jnp.dot(active, down_v[...], preferred_element_type=jnp.float32)
        answer = answer.astype(jnp.bfloat16)
        arecv[d, :slot] = answer[:slot]
        asend[d, slot:] = answer[slot:]
        for o in range(1, peers):
            acopy(d, o).start()

    def combine(d):
        for o in range(1, peers):
            acopy(d, o).wait_recv()
        at, shares = places(d)
        mix = jnp.where(at[0], shares[0], 0.0) + jnp.where(at[1], shares[1], 0.0)
        high = mix.astype(jnp.bfloat16)
        low = (mix - high.astype(jnp.float32)).astype(jnp.bfloat16)
        dims = (((0,), (0,)), ((), ()))
        answers = arecv[d]
        total = lax.dot_general(high, answers, dims, preferred_element_type=jnp.float32)
        total += lax.dot_general(low, answers, dims, preferred_element_type=jnp.float32)
        if d == 0:
            cret[0] = total.astype(jnp.bfloat16)
        else:
            csend[d] = total.astype(jnp.bfloat16)
            ccopy(d).start()

    a, b, c = ORDER
    entry(0)
    entry(a)
    for copy in weights:
        copy.wait()
    expert(0)
    entry(b)
    expert(a)
    combine(0)
    entry(c)
    combine(a)
    expert(b)
    combine(b)
    expert(c)
    combine(c)

    for d in ORDER:
        ccopy(d).wait_recv()
    dims = (((0,), (0,)), ((), ()))
    gathered = cret[...].reshape(PLANES * group_rows, cret.shape[2])
    total = lax.dot_general(place_ref[...], gathered, dims, preferred_element_type=jnp.float32)
    out_ref[...] = (hidden_ref[...].astype(jnp.float32) + total).astype(jnp.bfloat16)

    for d in ORDER:
        mcopy(d).wait_send()
        zcopy(d).wait_send()
        ccopy(d).wait_send()
    for d in range(PLANES):
        for o in range(1, peers):
            xcopy(d, o).wait_send()
            acopy(d, o).wait_send()


def moe(normed, hidden, place, meta, gate_weight, up_weight, down_weight, cap):
    rows, width = normed.shape
    peers = lax.axis_size("sp") // PLANES * lax.axis_size("tp")
    group_rows = place.shape[0] // PLANES
    slot = max(cap, ROWS_MIN)
    slots = peers * slot
    bf16 = jnp.bfloat16
    vmem = pl.BlockSpec(memory_space=pltpu.VMEM)
    hbm = pl.BlockSpec(memory_space=pl.ANY)
    dma = pltpu.SemaphoreType.DMA
    return pl.pallas_call(
        functools.partial(moe_kernel, cap, slot),
        out_shape=jax.ShapeDtypeStruct((rows, width), bf16),
        in_specs=[vmem] * 4 + [hbm] * 3,
        out_specs=vmem,
        scratch_shapes=[
            pltpu.VMEM((PLANES, group_rows, width), bf16),
            pltpu.VMEM((PLANES, group_rows, width), bf16),
            pltpu.VMEM(meta.shape, jnp.float32),
            pltpu.VMEM((PLANES, slots, width), bf16),
            pltpu.VMEM((PLANES, slots, width), bf16),
            pltpu.VMEM((PLANES, slots, width), bf16),
            pltpu.VMEM((PLANES, slots, width), bf16),
            pltpu.VMEM((PLANES, group_rows, width), bf16),
            pltpu.VMEM((PLANES, group_rows, width), bf16),
            pltpu.VMEM(gate_weight.shape[1:], bf16),
            pltpu.VMEM(up_weight.shape[1:], bf16),
            pltpu.VMEM(down_weight.shape[1:], bf16),
            dma((3,)),
            dma((PLANES,)),
            dma((PLANES,)),
            dma((PLANES,)),
            dma((PLANES,)),
            dma((PLANES, peers)),
            dma((PLANES, peers)),
            dma((PLANES, peers)),
            dma((PLANES, peers)),
            dma((PLANES,)),
            dma((PLANES,)),
        ],
        compiler_params=pltpu.CompilerParams(
            collective_id=0, has_side_effects=True, vmem_limit_bytes=60 * 1024 * 1024
        ),
    )(normed, hidden, place, meta, gate_weight, up_weight, down_weight)


def routing(expert_pick, pair_logits, group_prob, cap):
    tokens = expert_pick.shape[0]
    chips = lax.axis_size("sp") // PLANES
    peers = chips * lax.axis_size("tp")
    group_rows = peers * cap // 2
    z = lax.axis_index("sp") // chips
    order = jnp.arange(tokens, dtype=jnp.int32)
    earlier = order[:, None] < order[None, :]
    picks = [expert_pick[:, 0], expert_pick[:, 1]]
    ranks = []
    for pick in picks:
        same = (picks[0][:, None] == pick[None, :]) | (picks[1][:, None] == pick[None, :])
        ranks.append(jnp.sum((same & earlier).astype(jnp.int32), axis=0))
    group = picks[0] // peers
    row = jnp.sum(((group[:, None] == group[None, :]) & earlier).astype(jnp.int32), axis=0)
    at = (group ^ z) * group_rows + row
    rows = jnp.arange(PLANES * group_rows, dtype=jnp.int32)
    hit = rows[:, None] == at[None, :]
    place = hit.astype(jnp.bfloat16)
    slot = max(cap, ROWS_MIN)
    first = group_prob * jax.nn.sigmoid(pair_logits[:, 0] - pair_logits[:, 1])
    second = group_prob * jax.nn.sigmoid(pair_logits[:, 1] - pair_logits[:, 0])
    fields = [(picks[k] % peers * slot + ranks[k] + 1).astype(jnp.float32) for k in range(2)]
    fields = [jnp.sum(jnp.where(hit, f[None, :], 0.0), axis=1) for f in fields + [first, second]]
    fields = [jnp.where(f > 0, f - 1.0, 65536.0) for f in fields[:2]] + fields[2:]
    meta = jnp.stack(fields).reshape(len(fields), PLANES, group_rows)
    meta = jnp.pad(meta, ((0, 8 - len(fields)), (0, 0), (0, 128 - group_rows)))
    return place, meta.transpose(1, 0, 2)


def local(
    glu_value,
    glu_gate,
    conv_kernel,
    conv_bias,
    group_gain,
    group_shift,
    out_weight,
    residual,
    ffn_gain,
    expert_pick,
    pair_logits,
    group_prob,
    gate_weight,
    up_weight,
    down_weight,
):
    glued_rows = (
        glu_value.astype(jnp.float32) * jax.nn.sigmoid(glu_gate.astype(jnp.float32))
    ).astype(jnp.bfloat16)
    reach_rows = conv_kernel.shape[0] - 1
    length = glued_rows.shape[0]
    earlier = from_behind(glued_rows[length - reach_rows :], "sp", 1)
    extended = jnp.concatenate([earlier, glued_rows], axis=0).astype(jnp.float32)
    kernel = conv_kernel.astype(jnp.float32)
    summed = jnp.zeros(glued_rows.shape, jnp.float32) + conv_bias
    for offset in range(reach_rows + 1):
        summed = summed + kernel[offset] * extended[offset : offset + length]
    groups_here = CONV_GROUPS // lax.axis_size("tp")
    grouped = summed.reshape(length, groups_here, -1)
    centre = jnp.mean(grouped, axis=-1, keepdims=True)
    variance = jnp.mean(jnp.square(grouped - centre), axis=-1, keepdims=True)
    leveled = ((grouped - centre) * lax.rsqrt(variance + EPS)).reshape(length, -1)
    mixed_rows = jax.nn.silu(leveled * group_gain + group_shift).astype(jnp.bfloat16)
    local_rows = residual.shape[0]
    regrouped = lax.all_to_all(mixed_rows, "tp", split_axis=0, concat_axis=1, tiled=True)
    projected = jnp.dot(regrouped, out_weight, preferred_element_type=jnp.float32)
    hidden = (residual.astype(jnp.float32) + projected).astype(jnp.bfloat16)
    hidden_full = hidden.astype(jnp.float32)
    scale_rows = lax.rsqrt(jnp.mean(hidden_full * hidden_full, axis=-1, keepdims=True) + EPS)
    normed = (hidden_full * scale_rows * ffn_gain).astype(jnp.bfloat16)
    experts_all = lax.axis_size("sp") * lax.axis_size("tp")
    capacity = 4 * local_rows // experts_all
    place, meta = routing(expert_pick, pair_logits, group_prob, capacity)
    return moe(normed, hidden, place, meta, gate_weight, up_weight, down_weight, capacity)


def solution(mesh):
    in_specs = (
        P("sp", "tp"),
        P("sp", "tp"),
        P(None, "tp"),
        P("tp"),
        P("tp"),
        P("tp"),
        P(),
        P(("sp", "tp"), None),
        P(),
        P(("sp", "tp"), None),
        P(("sp", "tp"), None),
        P(("sp", "tp")),
        P(("sp", "tp"), None, None),
        P(("sp", "tp"), None, None),
        P(("sp", "tp"), None, None),
    )
    out_specs = P(("sp", "tp"), None)
    return jax.shard_map(local, mesh=mesh, in_specs=in_specs, out_specs=out_specs, check_vma=False)
```

time: 160 us -> 106 us (0.66)
  Pallas kernels: 0 us -> 75 us
  blocking collectives: 57.5 us -> 3.94 us
  waiting for transfers between devices: 48.7 us -> 0.01 us
  local copies, waits for them, and re-layouts: 22.7 us -> 5.29 us
  matrix products: 10.2 us -> 3.03 us
  starting transfers between devices: 8.67 us -> 4.87 us
  other arithmetic: 11 us -> 13.1 us
    pallas_call x0 -> x1, Pallas kernels: none -> 75 us  [moe(): pl.pallas_call(functools.partial(moe_kernel, cap, slot), out_shape=jax.Sh...]
    all_to_all x1 -> x0, blocking collectives: 53.6 us -> none  [local(): lax.all_to_all(outgoing, ('sp', 'tp'), split_axis=0, concat_axis=0, tiled...]
    all_to_all x1 -> x0, waiting for transfers between devices: 48.7 us -> none  [local(): lax.all_to_all(answer.reshape(senders, slot_count, width_here), ('sp', 't...]
    dot_general x2 -> x0, matrix products: 7.21 us -> none  [the longest x1 5.96 us: local(): jnp.dot(active, down_weight[0], preferred_element_type=jnp.float32)]
    gather x1 -> x0, local copies, waits for them, and re-layouts: 5.21 us -> none  [local(): picked = flat_returned[slot_place].reshape(local_rows, picks, model_width)]
    scatter x1 -> x0, local copies, waits for them, and re-layouts: 4.43 us -> none  [local(): jnp.zeros((experts_all * capacity, model_width), jnp.bfloat16)]
    all_to_all x1 -> x0, starting transfers between devices: 3.79 us -> none  [local(): lax.all_to_all(answer.reshape(senders, slot_count, width_here), ('sp', 't...]
    reshape x2 -> x0, local copies, waits for them, and re-layouts: 2.98 us -> none  [the longest x1 1.74 us: local(): picked = flat_returned[slot_place].reshape(local_rows, picks, model_width)]
  transfers between devices with their start and end apart: 2 -> 1, of which waited for: 1 -> 0; matrix products, arithmetic and copies ran while one was open for 3% -> 7% of each run, Pallas kernels for 0% -> 0%
where the time goes in v1:
time: 106 us; the launch traced here: 105 us
  Pallas kernels  75 us (71%)
  other arithmetic  13.1 us (12%)
  local copies, waits for them, and re-layouts  5.29 us (5%)
  starting transfers between devices  4.87 us (5%)
  blocking collectives  3.94 us (4%)
  matrix products  3.03 us (3%)
    pallas_call x1, Pallas kernels, moe(): pl.pallas_call(functools.partial(moe_kernel, cap, slot), out_shape=jax.Sh...  75 us
    ppermute x1, starting transfers between devices, from_behind(): return lax.ppermute(value, axis, pairs)  4.87 us
    all_to_all x1, blocking collectives, local(): lax.all_to_all(mixed_rows, 'tp', split_axis=0, concat_axis=1, tiled=True)  3.94 us
    dot_general x1, matrix products, local(): jnp.dot(regrouped, out_weight, preferred_element_type=jnp.float32)  3.03 us
    add x1, other arithmetic, local(): summed = summed + kernel[offset] * extended[offset:offset + length]  2.8 us
    convert_element_type x1, other arithmetic, local(): jax.nn.silu(leveled * group_gain + group_shift).astype(jnp.bfloat16)  2.3 us
  transfers between devices with their start and end apart: 1, of which 0 were waited for; matrix products, arithmetic and copies ran while one was open for 7% of the time, Pallas kernels for 0%

profile of v1, /device:TPU:0, one launch (start us, length us, event | category | flops | bytes accessed | tf_op | source)
XLA Modules:
  0.0 105.4 jit_solution(4967277526230133652)
XLA Ops:
  0.0 1.2 %multiply_convert_fusion.1 = bf16[256,512]{1,0:T(8,128)(2,1)S(1)} fusion(bf16[256,512]{1,0:T(8,128)(2,1)} %param.16, bf16[256,512]{1,0:T(8,128)(2,1)} %param.15), kind=kLoop, calls=%fused_computation.75 | loop fusion | flops 917504 | bytes 786432 | tf_op jit(solution)/shard_map/convert_element_type | solution.py:332
  1.2 4.9 %collective-permute-start = (bf16[30,512]{1,0:T(8,128)(2,1)S(1)}, bf16[30,512]{1,0:T(8,128)(2,1)S(1)}, u32[]{:S(2)}, u32[]{:S(2)}) collective-permute-start(bf16[30,512]{1,0:T(8,128)(2,1)S(1)} %slice.271), channel_id=1, source_target_pairs={{0,2},{2,4},{4,6},{6,8},{8,10},{10,12},{12,14},{14,16},{16,18},{18... | collective-permute-start | bytes 92168 | tf_op jit(solution)/shard_map/ppermute | solution.py:19
  6.1 1.0 fusion.48
  7.1 1.0 fusion.49
  8.1 0.8 fusion.47
  8.9 0.1 convert_reduce_fusion.1
  9.0 0.8 add_convert_fusion.1
  9.8 0.7 and_select_fusion.3
  10.5 0.1 convert_reduce_fusion.2
  10.6 0.6 fusion.37.place_ref
  11.2 0.8 bitcast_multiply_fusion.2
  12.0 0.2 select_reduce_fusion.3
  12.2 0.1 select_n.86
  12.3 0.1 select_n.90
  12.4 0.1 stack.11
  12.5 0.1 stack.12
  12.6 0.6 fusion.41.meta_ref
  13.2 0.0 collective-permute-done
  13.2 0.1 maximum_convert_fusion
  13.3 2.8 %fusion.6 = f32[256,512]{1,0:T(8,128)S(1)} fusion(f32[286,512]{1,0:T(8,128)S(1)} %maximum_convert_fusion, f32[512]{0:T(512)S(1)} %bitcast.136, f32[512]{0:T(512)S(1)} %bitcast.134, f32[512]{0:T(512)S(1)} %bitcast.132, f32[512]{0:T(512)S(1)} %bitcast.130, f32[512]{0:T(512)S(1)} %bitcast.128, f32[512]{0:T(512)S(1)} %bitcast.126, f32[512]{0:T(512)S(1)} %bitcast.124, ...), kind=kLoop, calls=%fused_computation.12 | loop fusion | flops 8126464 | bytes 16842752 | tf_op jit(solution)/shard_map/add | solution.py:340
  16.1 0.0 copy-start.3
  16.1 0.0 copy-start.4
  16.1 0.0 copy-start.5
  16.1 0.2 reshape.208
  16.3 0.3 reduce_sum.90
  16.7 0.6 multiply_reduce_fusion
  17.3 0.3 mul.479
  17.7 0.3 sub.43
  18.0 0.0 copy-done.3
  18.0 0.0 copy-done.4
  18.0 0.0 copy-done.5
  18.0 0.0 copy-start.1
  18.1 2.3 %multiply_convert_fusion = bf16[256,512]{1,0:T(8,128)(2,1)S(1)} fusion(f32[32,8,4,128]{3,2,1,0:T(4,128)S(1)} %bitcast.71, f32[32,8,4,128]{3,2,1,0:T(4,128)S(1)} %bitcast.72, f32[512]{0:T(512)S(1)} %copy-done.4, f32[512]{0:T(512)S(1)} %copy-done.5, f32[286,512]{1,0:T(8,128)S(1)} %maximum_convert_fusion, f32[512]{0:T(512)S(1)} %bitcast.137, ...), kind=kLoop, calls=%fused_computation.73 | loop fusion | flops 9306112 | bytes 17633280 | tf_op jit(solution)/shard_map/convert_element_type | solution.py:346
  20.4 0.0 copy-start.2
  20.4 3.9 %all_to_all.19 = bf16[2,128,512]{2,1,0:T(8,128)(2,1)S(1)} all-to-all(bf16[2,128,512]{2,1,0:T(8,128)(2,1)S(1)} %bitcast.73), channel_id=1, replica_groups=mesh['sp'=16,'tp'=2] {'tp'}, dimensions={0} | all-to-all | bytes 524288 | tf_op jit(solution)/shard_map/all_to_all | solution.py:348
  24.3 0.2 copy.17
  24.5 0.0 copy-done.1
  24.5 3.0 %fusion.1 = (f32[128]{0:T(128)S(1)}, bf16[128,2048]{1,0:T(8,128)(2,1)S(1)}) fusion(bf16[128,1024]{0,1:T(8,128)(2,1)S(1)} %bitcast.74, bf16[1024,2048]{1,0:T(8,128)(2,1)} %param.21, bf16[128,2048]{1,0:T(8,128)(2,1)S(1)} %copy-done.1), kind=kOutput, calls=%fused_computation.4 | convolution fusion | flops 538443648 | bytes 5505536 | tf_op jit(solution)/shard_map/dot_general | solution.py:349
  27.5 0.0 copy-start
  27.6 0.0 copy-done.2
  27.6 1.0 fusion.3.normed_ref
  28.5 0.0 copy-done
  28.5 75.0 %shard_map.145 = bf16[128,2048]{1,0:T(8,128)(2,1)} custom-call(bf16[128,2048]{1,0:T(8,128)(2,1)} %fusion.3.normed_ref, bf16[128,2048]{1,0:T(8,128)(2,1)} %copy-done, bf16[256,128]{1,0:T(8,128)(2,1)} %fusion.37.place_ref, f32[4,8,128]{2,1,0:T(8,128)} %fusion.41.meta_ref, bf16[1,2048,512]{2,1,0:T(8,128)(2,1)} %gate_hbm.1, bf16[1,2048,512]{2,1,0:T(8,128)(2,1)} %up_hbm.1, ...), custom_call_target="tpu_custom_call" | custom-call | tf_op jit(solution)/shard_map/pallas_call | solution.py:247
  103.6 1.9 %copy.27 = bf16[128,2048]{1,0:T(8,128)(2,1)} copy(bf16[128,2048]{1,0:T(8,128)(2,1)} %shard_map.145) | data formatting | bytes 1048576
  (6 shorter events, 0.1 us)
Async XLA Ops:
  1.2 12.0 %collective-permute-start = (bf16[30,512]{1,0:T(8,128)(2,1)S(1)}, bf16[30,512]{1,0:T(8,128)(2,1)S(1)}, u32[]{:S(2)}, u32[]{:S(2)}) collective-permute-start(bf16[30,512]{1,0:T(8,128)(2,1)S(1)} %slice.271), channel_id=1, source_target_pairs={{0,2},{2,4},{4,6},{6,8},{8,10},{10,12},{12,14},{14,16},{16,18},{18... | collective-permute-start | bytes 92168 | tf_op jit(solution)/shard_map/ppermute | solution.py:19
  16.1 1.9 %copy-start.3 = (f32[512]{0:T(512)S(1)}, f32[512]{0:T(512)}, u32[]{:S(2)}) copy-start(f32[512]{0:T(512)} %param.18) | copy-start | bytes 6148
  16.1 1.9 %copy-start.4 = (f32[512]{0:T(512)S(1)}, f32[512]{0:T(512)}, u32[]{:S(2)}) copy-start(f32[512]{0:T(512)} %param.20) | copy-start | bytes 6148
  16.1 1.9 %copy-start.5 = (f32[512]{0:T(512)S(1)}, f32[512]{0:T(512)}, u32[]{:S(2)}) copy-start(f32[512]{0:T(512)} %param.19) | copy-start | bytes 6148
  18.0 6.5 %copy-start.1 = (bf16[128,2048]{1,0:T(8,128)(2,1)S(1)}, bf16[128,2048]{1,0:T(8,128)(2,1)}, u32[]{:S(2)}) copy-start(bf16[128,2048]{1,0:T(8,128)(2,1)} %param.22) | copy-start | bytes 1572868
  20.4 7.2 %copy-start.2 = (f32[2048]{0:T(1024)S(1)}, f32[2048]{0:T(1024)}, u32[]{:S(2)}) copy-start(f32[2048]{0:T(1024)} %param.23) | copy-start | bytes 24580
  27.5 1.0 copy-start

commit v2 on v1

v2 whole, which is shorter than its diff:
```python
import functools

import jax
import jax.numpy as jnp
from jax import lax
from jax.experimental import pallas as pl
from jax.experimental.pallas import tpu as pltpu
from jax.sharding import PartitionSpec as P

CONV_GROUPS = 8


EPS = 1e-06


PLANES = 4
MESH = pl.DeviceIdType.MESH
ORDER = (1, 3, 2)
ROWS_MIN = 16


def layer_kernel(
    cap,
    slot,
    value_ref,
    gate_ref,
    taps_ref,
    bias_ref,
    gain_ref,
    shift_ref,
    residual_ref,
    ffn_ref,
    pick_ref,
    logit_ref,
    prob_ref,
    out_hbm,
    gate_hbm,
    up_hbm,
    down_hbm,
    out_ref,
    glued,
    hsend,
    hrecv,
    mixed,
    mrest,
    place_ref,
    meta_ref,
    normed_ref,
    hidden_ref,
    proj,
    out_v,
    zsend,
    zrecv,
    mrecv,
    xsend,
    xrecv,
    asend,
    arecv,
    csend,
    cret,
    gate_v,
    up_v,
    down_v,
    wsem,
    hss,
    hrs,
    tss,
    trs,
    zss,
    zrs,
    mss,
    mrs,
    xss,
    xrs,
    ass,
    ars,
    css,
    crs,
):
    n_tp = lax.axis_size("tp")
    chips = lax.axis_size("sp") // PLANES
    peers = chips * n_tp
    sp = lax.axis_index("sp")
    tp = lax.axis_index("tp")
    n_sp = lax.axis_size("sp")
    z = sp // chips
    here = sp % chips
    tokens = residual_ref.shape[0]
    length, channels = value_ref.shape
    reach = taps_ref.shape[0] - 1
    lead = hsend.shape[0]
    j = here * n_tp + tp
    slots = peers * slot
    group_rows = zsend.shape[1]

    def plane(d):
        if d == 1:
            return z + 1 - 2 * (z % 2)
        if d == 2:
            return z + 2 - 4 * (z // 2)
        return PLANES - 1 - z

    def mate(d):
        return (plane(d) * chips + here, tp)

    def peer(k):
        return (z * chips + k // n_tp, k % n_tp)

    def zcopy(d):
        return pltpu.make_async_remote_copy(
            src_ref=zsend.at[d], dst_ref=zrecv.at[d], send_sem=zss.at[d], recv_sem=zrs.at[d],
            device_id=mate(d), device_id_type=MESH,
        )

    def mcopy(d):
        return pltpu.make_async_remote_copy(
            src_ref=meta_ref.at[d], dst_ref=mrecv.at[d], send_sem=mss.at[d], recv_sem=mrs.at[d],
            device_id=mate(d), device_id_type=MESH,
        )

    def ccopy(d):
        return pltpu.make_async_remote_copy(
            src_ref=csend.at[d], dst_ref=cret.at[d], send_sem=css.at[d], recv_sem=crs.at[d],
            device_id=mate(d), device_id_type=MESH,
        )

    def xcopy(d, o):
        rows = pl.ds(o * slot, slot)
        return pltpu.make_async_remote_copy(
            src_ref=xsend.at[d, rows], dst_ref=xrecv.at[d, rows],
            send_sem=xss.at[d, o], recv_sem=xrs.at[d, o],
            device_id=peer((j + o) % peers), device_id_type=MESH,
        )

    def acopy(d, o):
        rows = pl.ds(o * slot, slot)
        return pltpu.make_async_remote_copy(
            src_ref=asend.at[d, rows], dst_ref=arecv.at[d, rows],
            send_sem=ass.at[d, o], recv_sem=ars.at[d, o],
            device_id=peer((j + peers - o) % peers), device_id_type=MESH,
        )

    def halo():
        return pltpu.make_async_remote_copy(
            src_ref=hsend, dst_ref=hrecv, send_sem=hss.at[0], recv_sem=hrs.at[0],
            device_id=((sp + 1) % n_sp, tp), device_id_type=MESH,
        )

    def tcopy(o):
        other = (tp + o) % n_tp
        rows = pl.ds(pl.multiple_of(other * tokens, tokens), tokens)
        return pltpu.make_async_remote_copy(
            src_ref=mixed.at[rows], dst_ref=mrest.at[o], send_sem=tss.at[o], recv_sem=trs.at[o],
            device_id=(sp, other), device_id_type=MESH,
        )

    out_copy = pltpu.make_async_copy(out_hbm, out_v, wsem.at[3])
    out_copy.start()
    weights = [
        pltpu.make_async_copy(gate_hbm.at[0], gate_v, wsem.at[0]),
        pltpu.make_async_copy(up_hbm.at[0], up_v, wsem.at[1]),
        pltpu.make_async_copy(down_hbm.at[0], down_v, wsem.at[2]),
    ]
    for copy in weights:
        copy.start()

    barrier = pltpu.get_barrier_semaphore()
    for d in ORDER:
        pl.semaphore_signal(barrier, inc=1, device_id=mate(d), device_id_type=MESH)
    for o in range(1, peers):
        pl.semaphore_signal(
            barrier, inc=1, device_id=peer((j + o) % peers), device_id_type=MESH
        )
    pl.semaphore_signal(
        barrier, inc=1, device_id=((sp + 1) % n_sp, tp), device_id_type=MESH
    )
    pl.semaphore_signal(
        barrier, inc=1, device_id=((sp + n_sp - 1) % n_sp, tp), device_id_type=MESH
    )

    f32 = jnp.float32
    bf16 = jnp.bfloat16
    block = 64
    for start in range(length - block, -1, -block):
        rows = slice(start, start + block)
        gated = value_ref[rows].astype(f32) / (1.0 + jnp.exp(-gate_ref[rows].astype(f32)))
        gated = gated.astype(bf16)
        glued[lead + start : lead + start + block] = gated.astype(f32)
        if start == length - block:
            hsend[...] = gated[block - lead :]
    pl.semaphore_wait(barrier, len(ORDER) + peers + 1)
    halo().start()

    lane = lax.broadcasted_iota(jnp.int32, (tokens, 128), 1)
    picks = pick_ref[...].astype(f32)
    logits = logit_ref[...]
    cols = [picks[:, 0:1], picks[:, 1:2], logits[:, 0:1], logits[:, 1:2]]
    wide = jnp.zeros((tokens, 128), f32)
    for k in range(4):
        wide = jnp.where(lane == k, cols[k], wide)
    tall = wide.T
    rows_of = [tall[k : k + 1, :] for k in range(4)]
    square = (tokens, tokens)
    earlier = lax.broadcasted_iota(jnp.int32, square, 0) < lax.broadcasted_iota(
        jnp.int32, square, 1
    )

    def group_of(pick):
        total = jnp.zeros(pick.shape, f32)
        for q in range(1, PLANES):
            total += jnp.where(pick >= (q * peers), 1.0, 0.0)
        return total

    def count(hit):
        return jnp.sum(jnp.where(hit & earlier, 1.0, 0.0), axis=0, keepdims=True)

    ranks = [count((cols[0] == r) | (cols[1] == r)) for r in rows_of[:2]]
    group_row = group_of(rows_of[0])
    spot = count(group_of(cols[0]) == group_row)
    away = group_row.astype(jnp.int32) ^ z
    at_row = away.astype(f32) * group_rows + spot
    row_id = lax.broadcasted_iota(jnp.int32, (PLANES * group_rows, tokens), 0).astype(f32)
    place_ref[...] = jnp.where(row_id == at_row, 1.0, 0.0).astype(bf16)
    gap = rows_of[2] - rows_of[3]
    shares = [prob_ref[...] / (1.0 + jnp.exp(-gap)), prob_ref[...] / (1.0 + jnp.exp(gap))]
    fields = [jnp.ones((1, tokens), f32)]
    for k in range(2):
        fields += [rows_of[k] - group_row * peers, ranks[k]]
    for share in shares:
        for _ in range(3):
            part = share.astype(bf16).astype(f32)
            fields.append(part)
            share = share - part
    field_id = lax.broadcasted_iota(jnp.int32, (16, tokens), 0)
    table = jnp.zeros((16, tokens), f32)
    for k, field in enumerate(fields):
        table = jnp.where(field_id == k, field, table)
    table = table.astype(bf16)
    meta_ref[...] = jnp.zeros(meta_ref.shape, f32)
    for d in range(PLANES):
        part = lax.dot_general(
            table,
            place_ref[d * group_rows : (d + 1) * group_rows, :],
            (((1,), (1,)), ((), ())),
            preferred_element_type=f32,
        )
        empty = (1.0 - part[0:1]) * 65536.0
        meta_ref[d, 0:1, :group_rows] = part[1:2] * slot + part[2:3] + empty
        meta_ref[d, 1:2, :group_rows] = part[3:4] * slot + part[4:5] + empty
        meta_ref[d, 2:3, :group_rows] = part[5:6] + part[6:7] + part[7:8]
        meta_ref[d, 3:4, :group_rows] = part[8:9] + part[9:10] + part[10:11]
    for d in ORDER:
        mcopy(d).start()

    wide_group = channels * n_tp // CONV_GROUPS
    taps = taps_ref[...].astype(f32)
    for start in range(length - block, -1, -block):
        if start == 0:
            halo().wait_recv()
            keep = jnp.where(sp > 0, 1.0, 0.0)
            glued[:lead] = hrecv[...].astype(f32) * keep
        for low_lane in range(0, channels, wide_group):
            part = slice(low_lane, low_lane + wide_group)
            total = jnp.zeros((block, wide_group), f32) + bias_ref[:, part]
            for offset in range(reach + 1):
                first = start + lead - reach + offset
                total += taps[offset : offset + 1, part] * glued[first : first + block, part]
            centre = jnp.mean(total, axis=-1, keepdims=True)
            total = total - centre
            variance = jnp.mean(total * total, axis=-1, keepdims=True)
            level = total * lax.rsqrt(variance + EPS)
            level = level * gain_ref[:, part] + shift_ref[:, part]
            mixed[start : start + block, part] = (level / (1.0 + jnp.exp(-level))).astype(bf16)
    for o in range(1, n_tp):
        tcopy(o).start()
    out_copy.wait()

    def weight_rows(which):
        return out_v[pl.ds(pl.multiple_of(which * channels, channels), channels), :]

    own = mixed[pl.ds(pl.multiple_of(tp * tokens, tokens), tokens), :]
    proj[...] = jnp.dot(own, weight_rows(tp), preferred_element_type=f32)
    for o in range(1, n_tp):
        tcopy(o).wait_recv()
        proj[...] += jnp.dot(
            mrest[o], weight_rows((tp + n_tp - o) % n_tp), preferred_element_type=f32
        )
    for start in range(0, tokens, 16):
        rows = slice(start, start + 16)
        hidden = (residual_ref[rows].astype(f32) + proj[rows]).astype(bf16)
        hidden_ref[rows] = hidden
        full = hidden.astype(f32)
        scale = lax.rsqrt(jnp.mean(full * full, axis=-1, keepdims=True) + EPS)
        normed_ref[rows] = (full * scale * ffn_ref[...]).astype(bf16)

    for d in ORDER + (0,):
        picked = jnp.dot(
            place_ref[d * group_rows : (d + 1) * group_rows, :],
            normed_ref[...],
            preferred_element_type=f32,
        )
        zsend[d] = picked.astype(bf16)
        if d:
            zcopy(d).start()

    def places(d):
        meta = meta_ref[0] if d == 0 else mrecv[d]
        row = lax.broadcasted_iota(jnp.int32, (slots, group_rows), 0).astype(jnp.float32)
        shift = (j * slot).astype(jnp.float32)
        out = []
        for k in range(2):
            at = meta[k : k + 1, :group_rows] - shift
            at = jnp.where(at < 0, at + slots, at)
            out.append(row == at)
        shares = [meta[2 + k : 3 + k, :group_rows] for k in range(2)]
        return out, shares

    def entry(d):
        if d:
            mcopy(d).wait_recv()
            zcopy(d).wait_recv()
        at, _ = places(d)
        chosen = jnp.where(at[0] | at[1], 1.0, 0.0).astype(jnp.bfloat16)
        rows = zsend[0] if d == 0 else zrecv[d]
        spread = jnp.dot(chosen, rows, preferred_element_type=jnp.float32).astype(jnp.bfloat16)
        xrecv[d, :slot] = spread[:slot]
        xsend[d, slot:] = spread[slot:]
        for o in range(1, peers):
            xcopy(d, o).start()

    def expert(d):
        for o in range(1, peers):
            xcopy(d, o).wait_recv()
        rows = xrecv[d]
        gate_out = jnp.dot(rows, gate_v[...], preferred_element_type=jnp.float32)
        up_out = jnp.dot(rows, up_v[...], preferred_element_type=jnp.float32)
        active = (gate_out / (1.0 + jnp.exp(-gate_out)) * up_out).astype(jnp.bfloat16)
        answer = jnp.dot(active, down_v[...], preferred_element_type=jnp.float32)
        answer = answer.astype(jnp.bfloat16)
        arecv[d, :slot] = answer[:slot]
        asend[d, slot:] = answer[slot:]
        for o in range(1, peers):
            acopy(d, o).start()

    def combine(d):
        for o in range(1, peers):
            acopy(d, o).wait_recv()
        at, shares = places(d)
        mix = jnp.where(at[0], shares[0], 0.0) + jnp.where(at[1], shares[1], 0.0)
        high = mix.astype(jnp.bfloat16)
        low = (mix - high.astype(jnp.float32)).astype(jnp.bfloat16)
        dims = (((0,), (0,)), ((), ()))
        answers = arecv[d]
        total = lax.dot_general(high, answers, dims, preferred_element_type=jnp.float32)
        total += lax.dot_general(low, answers, dims, preferred_element_type=jnp.float32)
        if d == 0:
            cret[0] = total.astype(jnp.bfloat16)
        else:
            csend[d] = total.astype(jnp.bfloat16)
            ccopy(d).start()

    a, b, c = ORDER
    entry(0)
    entry(a)
    for copy in weights:
        copy.wait()
    expert(0)
    entry(b)
    inner = (z >= 1) & (z < PLANES - 1)

    @pl.when(inner)
    def _():
        expert(a)
        combine(0)
        expert(b)
        combine(a)
        combine(b)
        entry(c)
        expert(c)
        combine(c)

    @pl.when(jnp.logical_not(inner))
    def _():
        expert(a)
        combine(0)
        entry(c)
        combine(a)
        expert(b)
        expert(c)
        combine(b)
        combine(c)

    for d in ORDER:
        ccopy(d).wait_recv()
    dims = (((0,), (0,)), ((), ()))
    gathered = cret[...].reshape(PLANES * group_rows, cret.shape[2])
    total = lax.dot_general(place_ref[...], gathered, dims, preferred_element_type=jnp.float32)
    out_ref[...] = (hidden_ref[...].astype(jnp.float32) + total).astype(jnp.bfloat16)

    halo().wait_send()
    for o in range(1, n_tp):
        tcopy(o).wait_send()
    for d in ORDER:
        mcopy(d).wait_send()
        zcopy(d).wait_send()
        ccopy(d).wait_send()
    for d in range(PLANES):
        for o in range(1, peers):
            xcopy(d, o).wait_send()
            acopy(d, o).wait_send()


def local(
    glu_value,
    glu_gate,
    conv_kernel,
    conv_bias,
    group_gain,
    group_shift,
    out_weight,
    residual,
    ffn_gain,
    expert_pick,
    pair_logits,
    group_prob,
    gate_weight,
    up_weight,
    down_weight,
):
    rows, width = residual.shape
    length, channels = glu_value.shape
    n_tp = lax.axis_size("tp")
    experts_all = lax.axis_size("sp") * n_tp
    cap = 4 * rows // experts_all
    peers = experts_all // PLANES
    group_rows = peers * cap // 2
    slot = max(cap, ROWS_MIN)
    slots = peers * slot
    lead = -(-(conv_kernel.shape[0] - 1) // 16) * 16
    bf16 = jnp.bfloat16
    f32 = jnp.float32
    vmem = pl.BlockSpec(memory_space=pltpu.VMEM)
    hbm = pl.BlockSpec(memory_space=pl.ANY)
    dma = pltpu.SemaphoreType.DMA
    return pl.pallas_call(
        functools.partial(layer_kernel, cap, slot),
        out_shape=jax.ShapeDtypeStruct((rows, width), bf16),
        in_specs=[vmem] * 11 + [hbm] * 4,
        out_specs=vmem,
        scratch_shapes=[
            pltpu.VMEM((lead + length, channels), f32),
            pltpu.VMEM((lead, channels), bf16),
            pltpu.VMEM((lead, channels), bf16),
            pltpu.VMEM((length, channels), bf16),
            pltpu.VMEM((n_tp, rows, channels), bf16),
            pltpu.VMEM((PLANES * group_rows, rows), bf16),
            pltpu.VMEM((PLANES, 8, 128), f32),
            pltpu.VMEM((rows, width), bf16),
            pltpu.VMEM((rows, width), bf16),
            pltpu.VMEM((rows, width), f32),
            pltpu.VMEM(out_weight.shape, bf16),
            pltpu.VMEM((PLANES, group_rows, width), bf16),
            pltpu.VMEM((PLANES, group_rows, width), bf16),
            pltpu.VMEM((PLANES, 8, 128), f32),
            pltpu.VMEM((PLANES, slots, width), bf16),
            pltpu.VMEM((PLANES, slots, width), bf16),
            pltpu.VMEM((PLANES, slots, width), bf16),
            pltpu.VMEM((PLANES, slots, width), bf16),
            pltpu.VMEM((PLANES, group_rows, width), bf16),
            pltpu.VMEM((PLANES, group_rows, width), bf16),
            pltpu.VMEM(gate_weight.shape[1:], bf16),
            pltpu.VMEM(up_weight.shape[1:], bf16),
            pltpu.VMEM(down_weight.shape[1:], bf16),
            dma((4,)),
            dma((1,)),
            dma((1,)),
            dma((n_tp,)),
            dma((n_tp,)),
            dma((PLANES,)),
            dma((PLANES,)),
            dma((PLANES,)),
            dma((PLANES,)),
            dma((PLANES, peers)),
            dma((PLANES, peers)),
            dma((PLANES, peers)),
            dma((PLANES, peers)),
            dma((PLANES,)),
            dma((PLANES,)),
        ],
        compiler_params=pltpu.CompilerParams(
            collective_id=0, has_side_effects=True, vmem_limit_bytes=62 * 1024 * 1024
        ),
    )(
        glu_value,
        glu_gate,
        conv_kernel,
        conv_bias[None, :],
        group_gain[None, :],
        group_shift[None, :],
        residual,
        ffn_gain[None, :],
        expert_pick,
        pair_logits,
        group_prob[None, :],
        out_weight,
        gate_weight,
        up_weight,
        down_weight,
    )


def solution(mesh):
    in_specs = (
        P("sp", "tp"),
        P("sp", "tp"),
        P(None, "tp"),
        P("tp"),
        P("tp"),
        P("tp"),
        P(),
        P(("sp", "tp"), None),
        P(),
        P(("sp", "tp"), None),
        P(("sp", "tp"), None),
        P(("sp", "tp")),
        P(("sp", "tp"), None, None),
        P(("sp", "tp"), None, None),
        P(("sp", "tp"), None, None),
    )
    out_specs = P(("sp", "tp"), None)
    return jax.shard_map(local, mesh=mesh, in_specs=in_specs, out_specs=out_specs, check_vma=False)
```

time: 106 us -> 82.8 us (0.78)
  other arithmetic: 13.1 us -> 0 us
  starting transfers between devices: 4.87 us -> 0 us
  blocking collectives: 3.94 us -> 0 us
  matrix products: 3.03 us -> 0 us
  Pallas kernels: 75 us -> 77.9 us
    convert_element_type x6 -> x0, other arithmetic: 5.95 us -> none  [the longest x1 2.3 us: local(): jax.nn.silu(leveled * group_gain + group_shift).astype(jnp.bfloat16)]
    ppermute x1 -> x0, starting transfers between devices: 4.87 us -> none  [from_behind(): return lax.ppermute(value, axis, pairs)]
    all_to_all x1 -> x0, blocking collectives: 3.94 us -> none  [local(): lax.all_to_all(mixed_rows, 'tp', split_axis=0, concat_axis=1, tiled=True)]
    dot_general x1 -> x0, matrix products: 3.03 us -> none  [local(): jnp.dot(regrouped, out_weight, preferred_element_type=jnp.float32)]
    pallas_call x1, Pallas kernels: 75 us -> 77.9 us  [local(): pl.pallas_call(functools.partial(layer_kernel, cap, slot), out_shape=jax....]
    add x2 -> x0, other arithmetic: 2.81 us -> none  [the longest x1 2.8 us: local(): summed = summed + kernel[offset] * extended[offset:offset + length]]
    unnamed x13 -> x3, local copies, waits for them, and re-layouts: 1.92 us -> 4.7 us
    slice x3 -> x0, local copies, waits for them, and re-layouts: 2.03 us -> none  [the longest x2 2.02 us: local(): summed = summed + kernel[offset] * extended[offset:offset + length]]
  transfers between devices with their start and end apart: 1 -> 0, of which waited for: 0 -> 0; matrix products, arithmetic and copies ran while one was open for 7% -> 0% of each run, Pallas kernels for 0% -> 0%
where the time goes in v2:
time: 82.8 us; the launch traced here: 82.6 us
  Pallas kernels  77.9 us (94%)
  local copies, waits for them, and re-layouts  4.7 us (6%)
    pallas_call x1, Pallas kernels, local(): pl.pallas_call(functools.partial(layer_kernel, cap, slot), out_shape=jax....  77.9 us
    unnamed x3, local copies, waits for them, and re-layouts  4.7 us

profile of v2, /device:TPU:0, one launch (start us, length us, event | category | flops | bytes accessed | tf_op | source)
XLA Modules:
  0.0 82.6 jit_solution(9767139423053980127)
XLA Ops:
  0.0 1.4 %copy.16.pick_ref = s32[128,2]{1,0:T(8,128)} copy(s32[128,2]{0,1:T(2,128)} %param.24) | data formatting | bytes 2048 | tf_op args[9]
  1.4 1.4 %copy.17.logit_ref = f32[128,2]{1,0:T(8,128)} copy(f32[128,2]{0,1:T(2,128)} %param.25) | data formatting | bytes 2048 | tf_op args[10]
  2.8 77.9 %shard_map.145 = bf16[128,2048]{1,0:T(8,128)(2,1)} custom-call(bf16[256,512]{1,0:T(8,128)(2,1)} %value_ref.1, bf16[256,512]{1,0:T(8,128)(2,1)} %gate_ref.1, bf16[31,512]{1,0:T(8,128)(2,1)} %taps_ref.1, f32[1,512]{1,0:T(1,128)} %bitcast.6, f32[1,512]{1,0:T(1,128)} %bitcast.7, f32[1,512]{1,0:T(1,128)} %bitcast.8, bf16[128,2048]{1,0:T(8,128)(2,1)} %residual_ref.1, ...), custom_call_target="tpu_custom_call" | custom-call | tf_op jit(solution)/shard_map/pallas_call | solution.py:445
  80.7 1.9 %copy.19 = bf16[128,2048]{1,0:T(8,128)(2,1)} copy(bf16[128,2048]{1,0:T(8,128)(2,1)} %shard_map.145) | data formatting | bytes 1048576

commit v3 on v2

--- a/solution.py
+++ b/solution.py
@@ -17,6 +17,7 @@
 MESH = pl.DeviceIdType.MESH
 ORDER = (1, 3, 2)
 ROWS_MIN = 16
+HALVES = 2
 
 
 def layer_kernel(
@@ -91,7 +92,11 @@
     lead = hsend.shape[0]
     j = here * n_tp + tp
     slots = peers * slot
-    group_rows = zsend.shape[1]
+    group_rows = zsend.shape[2]
+    half = zsend.shape[3]
+
+    def span(h):
+        return slice(h * half, (h + 1) * half)
 
     def plane(d):
         if d == 1:
@@ -106,9 +111,10 @@
     def peer(k):
         return (z * chips + k // n_tp, k % n_tp)
 
-    def zcopy(d):
-        return pltpu.make_async_remote_copy(
-            src_ref=zsend.at[d], dst_ref=zrecv.at[d], send_sem=zss.at[d], recv_sem=zrs.at[d],
+    def zcopy(d, h):
+        return pltpu.make_async_remote_copy(
+            src_ref=zsend.at[d, h], dst_ref=zrecv.at[d, h],
+            send_sem=zss.at[d, h], recv_sem=zrs.at[d, h],
             device_id=mate(d), device_id_type=MESH,
         )
 
@@ -118,25 +124,26 @@
             device_id=mate(d), device_id_type=MESH,
         )
 
-    def ccopy(d):
-        return pltpu.make_async_remote_copy(
-            src_ref=csend.at[d], dst_ref=cret.at[d], send_sem=css.at[d], recv_sem=crs.at[d],
+    def ccopy(d, h):
+        return pltpu.make_async_remote_copy(
+            src_ref=csend.at[d, h], dst_ref=cret.at[d, h],
+            send_sem=css.at[d, h], recv_sem=crs.at[d, h],
             device_id=mate(d), device_id_type=MESH,
         )
 
-    def xcopy(d, o):
+    def xcopy(d, h, o):
         rows = pl.ds(o * slot, slot)
         return pltpu.make_async_remote_copy(
-            src_ref=xsend.at[d, rows], dst_ref=xrecv.at[d, rows],
-            send_sem=xss.at[d, o], recv_sem=xrs.at[d, o],
+            src_ref=xsend.at[d, h, rows], dst_ref=xrecv.at[d, h, rows],
+            send_sem=xss.at[d, h, o], recv_sem=xrs.at[d, h, o],
             device_id=peer((j + o) % peers), device_id_type=MESH,
         )
 
-    def acopy(d, o):
+    def acopy(d, h, o):
         rows = pl.ds(o * slot, slot)
         return pltpu.make_async_remote_copy(
-            src_ref=asend.at[d, rows], dst_ref=arecv.at[d, rows],
-            send_sem=ass.at[d, o], recv_sem=ars.at[d, o],
+            src_ref=asend.at[d, h, rows], dst_ref=arecv.at[d, h, rows],
+            send_sem=ass.at[d, h, o], recv_sem=ars.at[d, h, o],
             device_id=peer((j + peers - o) % peers), device_id_type=MESH,
         )
 
@@ -294,14 +301,15 @@
         normed_ref[rows] = (full * scale * ffn_ref[...]).astype(bf16)
 
     for d in ORDER + (0,):
-        picked = jnp.dot(
-            place_ref[d * group_rows : (d + 1) * group_rows, :],
-            normed_ref[...],
-            preferred_element_type=f32,
-        )
-        zsend[d] = picked.astype(bf16)
-        if d:
-            zcopy(d).start()
+        for h in range(HALVES):
+            picked = jnp.dot(
+                place_ref[d * group_rows : (d + 1) * group_rows, :],
+                normed_ref[:, span(h)],
+                preferred_element_type=f32,
+            )
+            zsend[d, h] = picked.astype(bf16)
+            if d:
+                zcopy(d, h).start()
 
     def places(d):
         meta = meta_ref[0] if d == 0 else mrecv[d]
@@ -318,46 +326,55 @@
     def entry(d):
         if d:
             mcopy(d).wait_recv()
-            zcopy(d).wait_recv()
         at, _ = places(d)
         chosen = jnp.where(at[0] | at[1], 1.0, 0.0).astype(jnp.bfloat16)
-        rows = zsend[0] if d == 0 else zrecv[d]
-        spread = jnp.dot(chosen, rows, preferred_element_type=jnp.float32).astype(jnp.bfloat16)
-        xrecv[d, :slot] = spread[:slot]
-        xsend[d, slot:] = spread[slot:]
-        for o in range(1, peers):
-            xcopy(d, o).start()
+        for h in range(HALVES):
+            if d:
+                zcopy(d, h).wait_recv()
+            rows = zsend[0, h] if d == 0 else zrecv[d, h]
+            spread = jnp.dot(chosen, rows, preferred_element_type=jnp.float32)
+            spread = spread.astype(jnp.bfloat16)
+            xrecv[d, h, :slot] = spread[:slot]
+            xsend[d, h, slot:] = spread[slot:]
+            for o in range(1, peers):
+                xcopy(d, h, o).start()
 
     def expert(d):
-        for o in range(1, peers):
-            xcopy(d, o).wait_recv()
-        rows = xrecv[d]
-        gate_out = jnp.dot(rows, gate_v[...], preferred_element_type=jnp.float32)
-        up_out = jnp.dot(rows, up_v[...], preferred_element_type=jnp.float32)
+        gate_out = None
+        for h in range(HALVES):
+            for o in range(1, peers):
+                xcopy(d, h, o).wait_recv()
+            rows = xrecv[d, h]
+            gate_part = jnp.dot(rows, gate_v[span(h), :], preferred_element_type=jnp.float32)
+            up_part = jnp.dot(rows, up_v[span(h), :], preferred_element_type=jnp.float32)
+            gate_out = gate_part if h == 0 else gate_out + gate_part
+            up_out = up_part if h == 0 else up_out + up_part
         active = (gate_out / (1.0 + jnp.exp(-gate_out)) * up_out).astype(jnp.bfloat16)
-        answer = jnp.dot(active, down_v[...], preferred_element_type=jnp.float32)
-        answer = answer.astype(jnp.bfloat16)
-        arecv[d, :slot] = answer[:slot]
-        asend[d, slot:] = answer[slot:]
-        for o in range(1, peers):
-            acopy(d, o).start()
+        for h in range(HALVES):
+            answer = jnp.dot(active, down_v[:, span(h)], preferred_element_type=jnp.float32)
+            answer = answer.astype(jnp.bfloat16)
+            arecv[d, h, :slot] = answer[:slot]
+            asend[d, h, slot:] = answer[slot:]
+            for o in range(1, peers):
+                acopy(d, h, o).start()
 
     def combine(d):
-        for o in range(1, peers):
-            acopy(d, o).wait_recv()
         at, shares = places(d)
         mix = jnp.where(at[0], shares[0], 0.0) + jnp.where(at[1], shares[1], 0.0)
         high = mix.astype(jnp.bfloat16)
         low = (mix - high.astype(jnp.float32)).astype(jnp.bfloat16)
         dims = (((0,), (0,)), ((), ()))
-        answers = arecv[d]
-        total = lax.dot_general(high, answers, dims, preferred_element_type=jnp.float32)
-        total += lax.dot_general(low, answers, dims, preferred_element_type=jnp.float32)
-        if d == 0:
-            cret[0] = total.astype(jnp.bfloat16)
-        else:
-            csend[d] = total.astype(jnp.bfloat16)
-            ccopy(d).start()
+        for h in range(HALVES):
+            for o in range(1, peers):
+                acopy(d, h, o).wait_recv()
+            answers = arecv[d, h]
+            total = lax.dot_general(high, answers, dims, preferred_element_type=jnp.float32)
+            total += lax.dot_general(low, answers, dims, preferred_element_type=jnp.float32)
+            if d == 0:
+                cret[0, h] = total.astype(jnp.bfloat16)
+            else:
+                csend[d, h] = total.astype(jnp.bfloat16)
+                ccopy(d, h).start()
 
     a, b, c = ORDER
     entry(0)
@@ -390,24 +407,33 @@
         combine(b)
         combine(c)
 
-    for d in ORDER:
-        ccopy(d).wait_recv()
     dims = (((0,), (0,)), ((), ()))
-    gathered = cret[...].reshape(PLANES * group_rows, cret.shape[2])
-    total = lax.dot_general(place_ref[...], gathered, dims, preferred_element_type=jnp.float32)
-    out_ref[...] = (hidden_ref[...].astype(jnp.float32) + total).astype(jnp.bfloat16)
+    for h in range(HALVES):
+        total = hidden_ref[:, span(h)].astype(jnp.float32)
+        for d in (0,) + ORDER:
+            if d:
+                ccopy(d, h).wait_recv()
+            total += lax.dot_general(
+                place_ref[d * group_rows : (d + 1) * group_rows, :],
+                cret[d, h],
+                dims,
+                preferred_element_type=jnp.float32,
+            )
+        out_ref[:, span(h)] = total.astype(jnp.bfloat16)
 
     halo().wait_send()
     for o in range(1, n_tp):
         tcopy(o).wait_send()
     for d in ORDER:
         mcopy(d).wait_send()
-        zcopy(d).wait_send()
-        ccopy(d).wait_send()
+        for h in range(HALVES):
+            zcopy(d, h).wait_send()
+            ccopy(d, h).wait_send()
     for d in range(PLANES):
-        for o in range(1, peers):
-            xcopy(d, o).wait_send()
-            acopy(d, o).wait_send()
+        for h in range(HALVES):
+            for o in range(1, peers):
+                xcopy(d, h, o).wait_send()
+                acopy(d, h, o).wait_send()
 
 
 def local(
@@ -459,15 +485,15 @@
             pltpu.VMEM((rows, width), bf16),
             pltpu.VMEM((rows, width), f32),
             pltpu.VMEM(out_weight.shape, bf16),
-            pltpu.VMEM((PLANES, group_rows, width), bf16),
-            pltpu.VMEM((PLANES, group_rows, width), bf16),
+            pltpu.VMEM((PLANES, HALVES, group_rows, width // HALVES), bf16),
+            pltpu.VMEM((PLANES, HALVES, group_rows, width // HALVES), bf16),
             pltpu.VMEM((PLANES, 8, 128), f32),
-            pltpu.VMEM((PLANES, slots, width), bf16),
-            pltpu.VMEM((PLANES, slots, width), bf16),
-            pltpu.VMEM((PLANES, slots, width), bf16),
-            pltpu.VMEM((PLANES, slots, width), bf16),
-            pltpu.VMEM((PLANES, group_rows, width), bf16),
-            pltpu.VMEM((PLANES, group_rows, width), bf16),
+            pltpu.VMEM((PLANES, HALVES, slots, width // HALVES), bf16),
+            pltpu.VMEM((PLANES, HALVES, slots, width // HALVES), bf16),
+            pltpu.VMEM((PLANES, HALVES, slots, width // HALVES), bf16),
+            pltpu.VMEM((PLANES, HALVES, slots, width // HALVES), bf16),
+            pltpu.VMEM((PLANES, HALVES, group_rows, width // HALVES), bf16),
+            pltpu.VMEM((PLANES, HALVES, group_rows, width // HALVES), bf16),
             pltpu.VMEM(gate_weight.shape[1:], bf16),
             pltpu.VMEM(up_weight.shape[1:], bf16),
             pltpu.VMEM(down_weight.shape[1:], bf16),
@@ -476,16 +502,16 @@
             dma((1,)),
             dma((n_tp,)),
             dma((n_tp,)),
+            dma((PLANES, HALVES)),
+            dma((PLANES, HALVES)),
             dma((PLANES,)),
             dma((PLANES,)),
-            dma((PLANES,)),
-            dma((PLANES,)),
-            dma((PLANES, peers)),
-            dma((PLANES, peers)),
-            dma((PLANES, peers)),
-            dma((PLANES, peers)),
-            dma((PLANES,)),
-            dma((PLANES,)),
+            dma((PLANES, HALVES, peers)),
+            dma((PLANES, HALVES, peers)),
+            dma((PLANES, HALVES, peers)),
+            dma((PLANES, HALVES, peers)),
+            dma((PLANES, HALVES)),
+            dma((PLANES, HALVES)),
         ],
         compiler_params=pltpu.CompilerParams(
             collective_id=0, has_side_effects=True, vmem_limit_bytes=62 * 1024 * 1024

time: 82.8 us -> 80.9 us (0.977)
  Pallas kernels: 77.9 us -> 76 us
    pallas_call x1, Pallas kernels: 77.9 us -> 76 us  [local(): pl.pallas_call(functools.partial(layer_kernel, cap, slot), out_shape=jax....]
where the time goes in v3:
time: 80.9 us; the launch traced here: 80.7 us
  Pallas kernels  76 us (94%)
  local copies, waits for them, and re-layouts  4.7 us (6%)
    pallas_call x1, Pallas kernels, local(): pl.pallas_call(functools.partial(layer_kernel, cap, slot), out_shape=jax....  76 us
    unnamed x3, local copies, waits for them, and re-layouts  4.7 us

profile of v3, /device:TPU:0, one launch (start us, length us, event | category | flops | bytes accessed | tf_op | source)
XLA Modules:
  0.0 80.7 jit_solution(15045234610261575073)
XLA Ops:
  0.0 1.4 %copy.16.pick_ref = s32[128,2]{1,0:T(8,128)} copy(s32[128,2]{0,1:T(2,128)} %param.24) | data formatting | bytes 2048 | tf_op args[9]
  1.4 1.4 %copy.17.logit_ref = f32[128,2]{1,0:T(8,128)} copy(f32[128,2]{0,1:T(2,128)} %param.25) | data formatting | bytes 2048 | tf_op args[10]
  2.8 76.0 %shard_map.145 = bf16[128,2048]{1,0:T(8,128)(2,1)} custom-call(bf16[256,512]{1,0:T(8,128)(2,1)} %value_ref.1, bf16[256,512]{1,0:T(8,128)(2,1)} %gate_ref.1, bf16[31,512]{1,0:T(8,128)(2,1)} %taps_ref.1, f32[1,512]{1,0:T(1,128)} %bitcast.6, f32[1,512]{1,0:T(1,128)} %bitcast.7, f32[1,512]{1,0:T(1,128)} %bitcast.8, bf16[128,2048]{1,0:T(8,128)(2,1)} %residual_ref.1, ...), custom_call_target="tpu_custom_call" | custom-call | tf_op jit(solution)/shard_map/pallas_call | solution.py:471
  78.8 1.9 %copy.19 = bf16[128,2048]{1,0:T(8,128)(2,1)} copy(bf16[128,2048]{1,0:T(8,128)(2,1)} %shard_map.145) | data formatting | bytes 1048576
